TPU v7x, 32 devices: a whole 2x2x4 slice. The times are simulated.
32 devices in a mesh: sp: 8 (over z, x), tp: 4 (over y, core).
Axes of the slice: x: 2, y: 2, z: 4, core: 2. Of those that a mesh axis runs over, the one named last changes fastest.
Arguments:
- queries: bfloat16 [1024, 2048], P('sp', 'tp'), may hold values from -440 to 440
- key_rows: bfloat16 [1024, 1024], P('sp', 'tp'), may hold values from -6 to 6
- value_rows: bfloat16 [1024, 1024], P('sp', 'tp'), may hold values from -6 to 6
- sink_logits: float32 [32], P('tp'), may hold values from -6 to 6
- out_weight: bfloat16 [2048, 2048], P('tp'), may hold values from -0.125 to 0.125
- residual: bfloat16 [1024, 2048], P('sp'), may hold values from -3 to 3
- norm_gain: float32 [2048], replicated, may hold values from 0.1 to 1.9
- routes: int32 [1024, 2], P('sp'), may hold values from 0 to 7, all different within a row; in each aligned block of 128 rows (0 to 127, 128 to 255, ...) at most 64 rows name the same one
- route_weights: float32 [1024, 2], P('sp'), may hold values from 0.2 to 1
- gate_weight: bfloat16 [8, 2048, 4096], P('sp', None, 'tp'), may hold values from -0.125 to 0.125
- up_weight: bfloat16 [8, 2048, 4096], P('sp', None, 'tp'), may hold values from -0.125 to 0.125
- down_weight: bfloat16 [8, 4096, 2048], P('sp', 'tp'), may hold values from -0.09375 to 0.09375
Outputs:
- layer_out: bfloat16 [1024, 2048], P('sp')
Inputs may be any that keep to these rules, and one draw needn't show every extreme that they name: `routes`: each row names 2 different experts. In each aligned block of 128 rows (the rows of one index of sp) no expert is named by more than 64 rows, a bound that some block reaches.
All inputs are finite; a program needn't handle non-finite values.
Results may differ from a plain program's by a relative error of at most 0.02.
Values may be sent and summed in bfloat16 or wider, within the bound.
A program may use at most 64 MiB of HBM per device.

v0:
```python
import jax
import jax.numpy as jnp
from jax import lax
from jax.sharding import PartitionSpec as P

HEAD_DIM = 64
QH = 32
WINDOW = 128
TOP = 2


def from_behind(array, axis, by):
    peers = lax.axis_size(axis)
    pairs = [(i, i + by) for i in range(peers) if 0 <= i + by < peers]
    return lax.ppermute(array, axis, pairs)


def per_device(
    queries,
    key_rows,
    value_rows,
    sink_logits,
    out_weight,
    residual,
    norm_gain,
    routes,
    route_weights,
    gate_weight,
    up_weight,
    down_weight,
):
    rows_here = queries.shape[0]
    width = residual.shape[1]
    heads_here = queries.shape[1] // HEAD_DIM
    kv_here = key_rows.shape[1] // HEAD_DIM
    group_size = heads_here // kv_here
    blocks = rows_here // WINDOW
    rim_rows = jnp.stack([key_rows, value_rows])
    before = from_behind(rim_rows, "sp", 1)
    key_ext = jnp.concatenate([before[0], key_rows], axis=0).reshape(
        blocks + 1, WINDOW, kv_here, HEAD_DIM
    )
    val_ext = jnp.concatenate([before[1], value_rows], axis=0).reshape(
        blocks + 1, WINDOW, kv_here, HEAD_DIM
    )
    key_pair = jnp.concatenate([key_ext[:-1], key_ext[1:]], axis=1)
    val_pair = jnp.concatenate([val_ext[:-1], val_ext[1:]], axis=1)
    query_blocks = queries.reshape(blocks, WINDOW, kv_here, group_size, HEAD_DIM)
    scores = jnp.einsum(
        "bqkgd,bckd->bkgqc", query_blocks, key_pair, preferred_element_type=jnp.float32
    ) * HEAD_DIM ** (-0.5)
    distance = jnp.arange(WINDOW)[:, None] + WINDOW - jnp.arange(2 * WINDOW)[None, :]
    offset = lax.axis_index("sp") * rows_here
    key_global = (
        offset
        + jnp.arange(blocks)[:, None, None] * WINDOW
        + jnp.arange(2 * WINDOW)[None, None, :]
        - WINDOW
    )
    allowed = (distance >= 0)[None] & (distance <= WINDOW)[None] & (key_global >= 0)
    head_ids = lax.axis_index("tp") * heads_here + jnp.arange(heads_here)
    slopes = jnp.exp2(-8.0 * (head_ids + 1).astype(jnp.float32) / QH).reshape(kv_here, group_size)
    scores = scores - slopes[None, :, :, None, None] * distance.astype(jnp.float32)
    scores = jnp.where(allowed[:, None, None], scores, -jnp.inf)
    row_peak = jnp.max(scores, axis=-1, keepdims=True)
    log_total = row_peak + jnp.log(jnp.sum(jnp.exp(scores - row_peak), axis=-1, keepdims=True))
    weights_bf = jnp.exp(scores - log_total).astype(jnp.bfloat16)
    attended = jnp.einsum(
        "bkgqc,bckd->bqkgd", weights_bf, val_pair, preferred_element_type=jnp.float32
    )
    keep_factor = jax.nn.sigmoid(
        log_total[..., 0] - sink_logits.reshape(kv_here, group_size)[None, :, :, None]
    )
    keep_factor = jnp.transpose(keep_factor, (0, 3, 1, 2))[..., None]
    attended = (
        (attended * keep_factor).astype(jnp.bfloat16).reshape(rows_here, heads_here * HEAD_DIM)
    )
    partial_value = jnp.dot(attended, out_weight, preferred_element_type=jnp.float32)
    partial_value = lax.optimization_barrier(partial_value.astype(jnp.bfloat16)).astype(jnp.float32)
    head_total = lax.psum(partial_value.astype(jnp.bfloat16), "tp").astype(jnp.float32)
    mixed_state = (residual.astype(jnp.float32) + head_total).astype(jnp.bfloat16)
    state32 = mixed_state.astype(jnp.float32)
    normed = (
        state32 * lax.rsqrt(jnp.mean(state32 * state32, axis=-1, keepdims=True) + 1e-06) * norm_gain
    ).astype(jnp.bfloat16)
    experts = lax.axis_size("sp")
    capacity = 2 * rows_here * TOP // experts
    flat_routes = routes.reshape(-1)
    member = (flat_routes[:, None] == jnp.arange(experts)[None, :]).astype(jnp.int32)
    slot_rank = jnp.sum((jnp.cumsum(member, axis=0) - 1) * member, axis=1)
    slot_index = flat_routes * capacity + slot_rank
    picker = (jnp.arange(experts * capacity)[:, None] == slot_index[None, :]).astype(jnp.int32)
    picker = jnp.sum(picker.reshape(experts * capacity, rows_here, TOP), axis=-1).astype(
        jnp.bfloat16
    )
    outgoing = (
        jnp.dot(picker, normed, preferred_element_type=jnp.float32)
        .astype(jnp.bfloat16)
        .reshape(experts, capacity, width)
    )
    w_gate = gate_weight[0]
    w_up = up_weight[0]
    w_down = down_weight[0]
    slot_share = capacity // lax.axis_size("tp")
    mine = lax.dynamic_slice_in_dim(outgoing, lax.axis_index("tp") * slot_share, slot_share, 1)
    arrived = lax.all_to_all(mine, "sp", split_axis=0, concat_axis=0, tiled=True)
    gathered = lax.all_gather(arrived, "tp", axis=1, tiled=True)
    flat_rows = gathered.reshape(-1, width)
    gate_pre = jnp.dot(flat_rows, w_gate, preferred_element_type=jnp.float32)
    up_pre = jnp.dot(flat_rows, w_up, preferred_element_type=jnp.float32)
    activated = (jax.nn.silu(gate_pre) * up_pre).astype(jnp.bfloat16)
    result = jnp.dot(activated, w_down, preferred_element_type=jnp.float32)
    result = lax.optimization_barrier(result.astype(jnp.bfloat16)).astype(jnp.float32)
    summed = lax.psum_scatter(
        result.reshape(gathered.shape).astype(jnp.bfloat16), "tp", scatter_dimension=1, tiled=True
    )
    back_rows = lax.all_to_all(summed, "sp", split_axis=0, concat_axis=0, tiled=True)
    returned = lax.all_gather(back_rows, "tp", axis=1, tiled=True)
    slot_table = returned.reshape(experts * capacity, width)
    picked = jnp.take(slot_table, slot_index, axis=0).reshape(rows_here, TOP, width)
    expert_mix = jnp.sum(route_weights[..., None] * picked.astype(jnp.float32), axis=1)
    return (state32 + expert_mix).astype(jnp.bfloat16)


def solution(mesh):
    placed = (
        P("sp", "tp"),
        P("sp", "tp"),
        P("sp", "tp"),
        P("tp"),
        P("tp", None),
        P("sp", None),
        P(),
        P("sp", None),
        P("sp", None),
        P("sp", None, "tp"),
        P("sp", None, "tp"),
        P("sp", "tp", None),
    )
    return jax.shard_map(
        per_device, mesh=mesh, in_specs=placed, out_specs=P("sp", None), check_vma=False
    )
```

profile of v0, /device:TPU:0, one launch (start us, length us, event | category | flops | bytes accessed | tf_op | source)
XLA Modules:
  0.0 208.5 jit_solution(12147156466361507940)
XLA Ops:
  6.5 1.0 pad_maximum_fusion
  7.6 4.9 %collective-permute-start = (bf16[2,128,256]{2,1,0:T(8,128)(2,1)S(1)}, bf16[2,128,256]{2,1,0:T(8,128)(2,1)S(1)}, u32[]{:S(2)}, u32[]{:S(2)}) collective-permute-start(bf16[2,128,256]{2,1,0:T(8,128)(2,1)S(1)} %pad_maximum_fusion), channel_id=1, source_target_pairs={{0,4},{4,8},{8,12},{12,16},{16,20},{20,24},{24,28},{1,5},{5,9},{9,... | collective-permute-start | bytes 393224 | tf_op jit(solution)/shard_map/ppermute | solution.py:15
  12.5 0.8 copy.50
  13.3 0.1 eq.40
  13.4 0.1 reshape.307
  13.7 0.6 reduce-window.6
  14.3 0.2 slice_reduce_fusion
  14.6 1.0 copy.46
  15.6 1.0 copy.44
  16.6 1.0 copy.47
  17.6 0.7 sub.85
  18.3 0.1 reduce_sum.51
  18.8 0.4 fusion.51
  19.3 0.2 exponential_reduce_fusion
  19.5 0.3 fusion.15
  19.9 1.3 convolution_convert_fusion.1
  21.3 33.7 %all-reduce.2.cloned.1.call-done = bf16[128,2048]{1,0:T(8,128)(2,1)} async-done(((bf16[128,2048]{1,0:T(8,128)(2,1)}), bf16[128,2048]{1,0:T(8,128)(2,1)}) %all-reduce.2.cloned.1.call-update) | async-done | bytes 524304 | tf_op jit(solution)/shard_map/psum | solution.py:80
  55.0 1.3 fusion.16
  56.3 1.8 convolution_convert_fusion
  58.2 18.9 %all_to_all.10 = bf16[8,16,2048]{2,1,0:T(8,128)(2,1)} all-to-all(bf16[8,16,2048]{2,1,0:T(8,128)(2,1)S(1)} %constant_dynamic-slice_fusion), channel_id=1, replica_groups=mesh['sp'=8,'tp'=4] {'sp'}, dimensions={0} | all-to-all | bytes 1048576 | tf_op jit(solution)/shard_map/all_to_all | solution.py:106
  77.2 21.3 %all-gather.3.cloned.1.call-done = bf16[8,64,2048]{2,1,0:T(8,128)(2,1)} async-done(((bf16[8,16,2048]{2,1,0:T(8,128)(2,1)}), bf16[8,64,2048]{2,1,0:T(8,128)(2,1)}) %all-gather.3.cloned.1.call-update) | async-done | bytes 2097168 | tf_op jit(solution)/shard_map/all_gather | solution.py:107
  98.5 6.5 %fusion.4 = f32[512,1024]{1,0:T(8,128)} fusion(bf16[512,2048]{1,0:T(8,128)(2,1)} %bitcast.102, bf16[1,2048,1024]{2,1,0:T(8,128)(2,1)} %param.21), kind=kOutput, calls=%fused_computation.5 | convolution fusion | flops 2147483648 | bytes 8388608 | tf_op jit(solution)/shard_map/dot_general | solution.py:109
  105.0 10.5 %fusion.6 = bf16[512,2048]{1,0:T(8,128)(2,1)} fusion(bf16[1,1024,2048]{2,1,0:T(8,128)(2,1)} %param.23, f32[512,1024]{1,0:T(8,128)} %fusion.4, bf16[512,2048]{1,0:T(8,128)(2,1)} %bitcast.103, bf16[1,2048,1024]{2,1,0:T(8,128)(2,1)} %param.22), kind=kOutput, calls=%fused_computation.7 | convolution fusion | flops 4299161600 | bytes 14680064 | tf_op jit(solution)/shard_map/dot_general | solution.py:112
  115.6 31.3 %reduce-scatter.2.cloned.1.call-done = bf16[8,16,2048]{2,1,0:T(8,128)(2,1)} async-done(((bf16[8,64,2048]{2,1,0:T(8,128)(2,1)}), bf16[8,16,2048]{2,1,0:T(8,128)(2,1)}) %reduce-scatter.2.cloned.1.call-update) | async-done | bytes 524304 | tf_op jit(solution)/shard_map/reduce_scatter | solution.py:114
  146.9 20.0 %all_to_all.11 = bf16[8,16,2048]{2,1,0:T(8,128)(2,1)} all-to-all(bf16[8,16,2048]{2,1,0:T(8,128)(2,1)} %reduce-scatter.2.cloned.1.call-done), channel_id=1, replica_groups=mesh['sp'=8,'tp'=4] {'sp'}, dimensions={0} | all-to-all | bytes 1048576 | tf_op jit(solution)/shard_map/all_to_all | solution.py:117
  167.0 0.1 mul.138
  167.1 0.1 copy.53
  167.4 20.3 %all-gather.5.cloned.1.call-done = bf16[8,64,2048]{2,1,0:T(8,128)(2,1)} async-done(((bf16[8,16,2048]{2,1,0:T(8,128)(2,1)}), bf16[8,64,2048]{2,1,0:T(8,128)(2,1)}) %all-gather.5.cloned.1.call-update) | async-done | bytes 2097168 | tf_op jit(solution)/shard_map/all_gather | solution.py:118
  187.7 5.2 %gather_fusion = bf16[256,2048]{1,0:T(8,128)(2,1)} fusion(bf16[512,2048]{1,0:T(8,128)(2,1)} %bitcast.89, s32[1024]{0:T(1024)S(1)} %pad_clamp_fusion), kind=kCustom, calls=%fused_computation | custom fusion | bytes 2098176 | tf_op jit(solution)/shard_map/jit(_take)/gather | solution.py:120
  192.9 2.6 %gather.7 = bf16[128,2,2048]{2,1,0:T(2,128)(2,1)} reshape(bf16[256,2048]{1,0:T(8,128)(2,1)} %gather_fusion) | data formatting | bytes 2097152 | tf_op jit(solution)/shard_map/jit(_take)/gather | solution.py:120
  195.5 5.5 %multiply_reduce_fusion = f32[128,2048]{1,0:T(8,128)S(1)} fusion(bf16[128,2,2048]{2,1,0:T(2,128)(2,1)} %gather.7, pred[128,2]{1,0:T(8,128)(4,1)S(1)} %copy.53, f32[128,2]{1,0:T(8,128)S(1)} %copy.49), kind=kLoop, calls=%fused_computation.10 | loop fusion | flops 1835008 | bytes 2098432 | tf_op jit(solution)/shard_map/reduce_sum | solution.py:121
  201.0 1.0 fusion.19
  (44 shorter events, 1.3 us)
Async XLA Ops:
  6.5 13.3 %copy-start = (bf16[512,2048]{1,0:T(8,128)(2,1)S(1)}, bf16[512,2048]{1,0:T(8,128)(2,1)}, u32[]{:S(2)}) copy-start(bf16[512,2048]{1,0:T(8,128)(2,1)} %param.16) | copy-start | bytes 6291460
  6.5 48.5 %all-reduce.2.cloned.1.call-start = ((), (), s32[]{:S(2)}) async-start(), calls=%async_computation.3 | async-start | bytes 1048576 | tf_op jit(solution)/shard_map/psum | solution.py:80
  7.6 11.0 %collective-permute-start = (bf16[2,128,256]{2,1,0:T(8,128)(2,1)S(1)}, bf16[2,128,256]{2,1,0:T(8,128)(2,1)S(1)}, u32[]{:S(2)}, u32[]{:S(2)}) collective-permute-start(bf16[2,128,256]{2,1,0:T(8,128)(2,1)S(1)} %pad_maximum_fusion), channel_id=1, source_target_pairs={{0,4},{4,8},{8,12},{12,16},{16,20},{20,24},{24,28},{1,5},{5,9},{9,... | collective-permute-start | bytes 393224 | tf_op jit(solution)/shard_map/ppermute | solution.py:15
  19.5 1.7 copy-start.3
  19.8 35.2 %copy-start.1 = (bf16[128,2048]{1,0:T(8,128)(2,1)S(1)}, bf16[128,2048]{1,0:T(8,128)(2,1)}, u32[]{:S(2)}) copy-start(bf16[128,2048]{1,0:T(8,128)(2,1)} %param.17) | copy-start | bytes 1572868
  19.8 36.5 %copy-start.4 = (f32[2048]{0:T(1024)S(1)}, f32[2048]{0:T(1024)}, u32[]{:S(2)}) copy-start(f32[2048]{0:T(1024)} %param.18) | copy-start | bytes 24580
  21.2 77.3 %all-gather.3.cloned.1.call-start = ((), (), s32[]{:S(2)}) async-start(), calls=%async_computation.4 | async-start | bytes 2621440 | tf_op jit(solution)/shard_map/all_gather | solution.py:107
  77.2 69.7 %reduce-scatter.2.cloned.1.call-start = ((), (), s32[]{:S(2)}) async-start(), calls=%async_computation.5 | async-start | bytes 2621440 | tf_op jit(solution)/shard_map/reduce_scatter | solution.py:114
  115.5 51.8 %copy-start.5 = (f32[128,2]{0,1:T(2,128)S(1)}, f32[128,2]{0,1:T(2,128)}, u32[]{:S(2)}) copy-start(f32[128,2]{0,1:T(2,128)} %param.20) | copy-start | bytes 3076
  115.5 72.1 %all-gather.5.cloned.1.call-start = ((), (), s32[]{:S(2)}) async-start(), calls=%async_computation.6 | async-start | bytes 2621440 | tf_op jit(solution)/shard_map/all_gather | solution.py:118
  192.9 8.1 %copy-start.2 = (bf16[128,2048]{1,0:T(8,128)(2,1)S(1)}, bf16[128,2048]{1,0:T(8,128)(2,1)}, u32[]{:S(2)}) copy-start(bf16[128,2048]{1,0:T(8,128)(2,1)} %all-reduce.2.cloned.1.call-done) | copy-start | bytes 1572868
Sparse Core Ops, SparseCore 0:
  21.3 33.7 all-reduce.1
  77.3 21.1 all-gather.2
  115.7 31.1 reduce-scatter.1
  167.0 20.6 all-gather.4
where the time goes:
time: 209 us
  waiting for transfers between devices  107 us (51%)
  blocking collectives  38.9 us (19%)
  matrix products  20.8 us (10%)
  local copies, waits for them, and re-layouts  13.8 us (7%)
  between operations  13.4 us (6%)
  other arithmetic  10 us (5%)
  starting transfers between devices  5.01 us (2%)
    psum x1, waiting for transfers between devices, per_device(): lax.psum(partial_value.astype(jnp.bfloat16), 'tp').astype(jnp.float32)  33.7 us
    reduce_scatter x1, waiting for transfers between devices, per_device(): lax.psum_scatter(result.reshape(gathered.shape).astype(jnp.bfloat16), 'tp...  31.3 us
    all_gather x1, waiting for transfers between devices, per_device(): gathered = lax.all_gather(arrived, 'tp', axis=1, tiled=True)  21.3 us
    all_gather x1, waiting for transfers between devices, per_device(): returned = lax.all_gather(back_rows, 'tp', axis=1, tiled=True)  20.3 us
    all_to_all x1, blocking collectives, per_device(): lax.all_to_all(summed, 'sp', split_axis=0, concat_axis=0, tiled=True)  20 us
    all_to_all x1, blocking collectives, per_device(): lax.all_to_all(mine, 'sp', split_axis=0, concat_axis=0, tiled=True)  18.9 us
    dot_general x1, matrix products, per_device(): result = jnp.dot(activated, w_down, preferred_element_type=jnp.float32)  10.5 us
    gather x2, local copies, waits for them, and re-layouts, per_device(): jnp.take(slot_table, slot_index, axis=0).reshape(rows_here, TOP, width)  7.81 us
  transfers between devices with their start and end apart: 5, of which 4 were waited for; matrix products, arithmetic and copies ran while one was open for 3% of the time, Pallas kernels for 0%

commit v1 on v0

--- a/solution.py
+++ b/solution.py
@@ -77,7 +77,9 @@
     )
     partial_value = jnp.dot(attended, out_weight, preferred_element_type=jnp.float32)
     partial_value = lax.optimization_barrier(partial_value.astype(jnp.bfloat16)).astype(jnp.float32)
-    head_total = lax.psum(partial_value.astype(jnp.bfloat16), "tp").astype(jnp.float32)
+    head_total = jnp.sum(lax.all_gather(partial_value.astype(jnp.bfloat16), "tp"), axis=0).astype(
+        jnp.float32
+    )
     mixed_state = (residual.astype(jnp.float32) + head_total).astype(jnp.bfloat16)
     state32 = mixed_state.astype(jnp.float32)
     normed = (

time: 209 us -> 197 us (0.943)
  waiting for transfers between devices: 107 us -> 94.5 us
    psum x1 -> x0, waiting for transfers between devices: 33.7 us -> none  [per_device(): lax.psum(partial_value.astype(jnp.bfloat16), 'tp').astype(jnp.float32)]
    all_gather x0 -> x1, waiting for transfers between devices: none -> 22.1 us  [per_device(): lax.all_gather(partial_value.astype(jnp.bfloat16), 'tp')]
where the time goes in v1:
time: 197 us
  waiting for transfers between devices  94.5 us (48%)
  blocking collectives  40.3 us (20%)
  matrix products  19.8 us (10%)
  between operations  13.4 us (7%)
  local copies, waits for them, and re-layouts  13 us (7%)
  other arithmetic  11 us (6%)
  starting transfers between devices  5.01 us (3%)
    reduce_scatter x1, waiting for transfers between devices, per_device(): lax.psum_scatter(result.reshape(gathered.shape).astype(jnp.bfloat16), 'tp...  31.3 us
    all_gather x1, waiting for transfers between devices, per_device(): lax.all_gather(partial_value.astype(jnp.bfloat16), 'tp')  22.1 us
    all_gather x1, waiting for transfers between devices, per_device(): gathered = lax.all_gather(arrived, 'tp', axis=1, tiled=True)  20.8 us
    all_to_all x1, blocking collectives, per_device(): lax.all_to_all(mine, 'sp', split_axis=0, concat_axis=0, tiled=True)  20.3 us
    all_gather x1, waiting for transfers between devices, per_device(): returned = lax.all_gather(back_rows, 'tp', axis=1, tiled=True)  20.3 us
    all_to_all x1, blocking collectives, per_device(): lax.all_to_all(summed, 'sp', split_axis=0, concat_axis=0, tiled=True)  20 us
    dot_general x1, matrix products, per_device(): result = jnp.dot(activated, w_down, preferred_element_type=jnp.float32)  10.5 us
    gather x2, local copies, waits for them, and re-layouts, per_device(): jnp.take(slot_table, slot_index, axis=0).reshape(rows_here, TOP, width)  7.75 us
  transfers between devices with their start and end apart: 5, of which 4 were waited for; matrix products, arithmetic and copies ran while one was open for 3% of the time, Pallas kernels for 0%

profile of v1, /device:TPU:0, one launch (start us, length us, event | category | flops | bytes accessed | tf_op | source)
XLA Modules:
  0.0 197.0 jit_solution(14990933014268275141)
XLA Ops:
  6.5 1.0 pad_maximum_fusion
  7.6 4.9 %collective-permute-start = (bf16[2,128,256]{2,1,0:T(8,128)(2,1)S(1)}, bf16[2,128,256]{2,1,0:T(8,128)(2,1)S(1)}, u32[]{:S(2)}, u32[]{:S(2)}) collective-permute-start(bf16[2,128,256]{2,1,0:T(8,128)(2,1)S(1)} %pad_maximum_fusion), channel_id=1, source_target_pairs={{0,4},{4,8},{8,12},{12,16},{16,20},{20,24},{24,28},{1,5},{5,9},{9,... | collective-permute-start | bytes 393224 | tf_op jit(solution)/shard_map/ppermute | solution.py:15
  12.6 1.0 copy.46
  13.6 1.0 copy.44
  14.5 1.0 copy.47
  15.6 0.7 sub.85
  16.6 0.4 fusion.51
  17.0 0.2 exponential_reduce_fusion
  17.3 0.3 fusion.15
  17.6 1.3 convolution_convert_fusion.1
  19.1 0.1 eq.40
  19.2 0.1 reshape.307
  19.4 0.6 reduce-window.6
  20.0 0.2 slice_reduce_fusion
  20.3 0.1 reduce_sum.64
  20.6 22.1 %all-gather.9.cloned.1.call-done = bf16[512,2048]{1,0:T(8,128)(2,1)} async-done(((bf16[128,2048]{1,0:T(8,128)(2,1)}), bf16[512,2048]{1,0:T(8,128)(2,1)}) %all-gather.9.cloned.1.call-update) | async-done | bytes 2097168 | tf_op jit(solution)/shard_map/all_gather | solution.py:80
  42.7 2.0 %reduce_sum.62 = bf16[128,2048]{1,0:T(8,128)(2,1)S(1)} reduce(bf16[4,128,2048]{2,1,0:T(8,128)(2,1)} %bitcast.92, bf16[]{:T(256)} %constant.68.clone.1), dimensions={0}, to_apply=%region_2.3 | reduce | flops 786432 | bytes 2621442 | tf_op jit(solution)/shard_map/reduce_sum | solution.py:80
  44.8 0.3 fusion.16
  45.0 0.8 convolution_convert_fusion
  45.9 20.3 %all_to_all.10 = bf16[8,16,2048]{2,1,0:T(8,128)(2,1)} all-to-all(bf16[8,16,2048]{2,1,0:T(8,128)(2,1)S(1)} %constant_dynamic-slice_fusion), channel_id=1, replica_groups=mesh['sp'=8,'tp'=4] {'sp'}, dimensions={0} | all-to-all | bytes 1048576 | tf_op jit(solution)/shard_map/all_to_all | solution.py:108
  66.2 20.8 %all-gather.5.cloned.1.call-done = bf16[8,64,2048]{2,1,0:T(8,128)(2,1)} async-done(((bf16[8,16,2048]{2,1,0:T(8,128)(2,1)}), bf16[8,64,2048]{2,1,0:T(8,128)(2,1)}) %all-gather.5.cloned.1.call-update) | async-done | bytes 2097168 | tf_op jit(solution)/shard_map/all_gather | solution.py:109
  87.0 6.5 %fusion.4 = f32[512,1024]{1,0:T(8,128)} fusion(bf16[512,2048]{1,0:T(8,128)(2,1)} %bitcast.104, bf16[1,2048,1024]{2,1,0:T(8,128)(2,1)} %param.21), kind=kOutput, calls=%fused_computation.5 | convolution fusion | flops 2147483648 | bytes 8388608 | tf_op jit(solution)/shard_map/dot_general | solution.py:111
  93.5 10.5 %fusion.6 = bf16[512,2048]{1,0:T(8,128)(2,1)} fusion(bf16[1,1024,2048]{2,1,0:T(8,128)(2,1)} %param.23, f32[512,1024]{1,0:T(8,128)} %fusion.4, bf16[512,2048]{1,0:T(8,128)(2,1)} %bitcast.105, bf16[1,2048,1024]{2,1,0:T(8,128)(2,1)} %param.22), kind=kOutput, calls=%fused_computation.7 | convolution fusion | flops 4299161600 | bytes 14680064 | tf_op jit(solution)/shard_map/dot_general | solution.py:114
  104.1 31.3 %reduce-scatter.2.cloned.1.call-done = bf16[8,16,2048]{2,1,0:T(8,128)(2,1)} async-done(((bf16[8,64,2048]{2,1,0:T(8,128)(2,1)}), bf16[8,16,2048]{2,1,0:T(8,128)(2,1)}) %reduce-scatter.2.cloned.1.call-update) | async-done | bytes 524304 | tf_op jit(solution)/shard_map/reduce_scatter | solution.py:116
  135.4 20.0 %all_to_all.11 = bf16[8,16,2048]{2,1,0:T(8,128)(2,1)} all-to-all(bf16[8,16,2048]{2,1,0:T(8,128)(2,1)} %reduce-scatter.2.cloned.1.call-done), channel_id=1, replica_groups=mesh['sp'=8,'tp'=4] {'sp'}, dimensions={0} | all-to-all | bytes 1048576 | tf_op jit(solution)/shard_map/all_to_all | solution.py:119
  155.5 0.1 mul.138
  155.7 0.1 copy.53
  155.9 20.3 %all-gather.7.cloned.1.call-done = bf16[8,64,2048]{2,1,0:T(8,128)(2,1)} async-done(((bf16[8,16,2048]{2,1,0:T(8,128)(2,1)}), bf16[8,64,2048]{2,1,0:T(8,128)(2,1)}) %all-gather.7.cloned.1.call-update) | async-done | bytes 2097168 | tf_op jit(solution)/shard_map/all_gather | solution.py:120
  176.2 5.2 %gather_fusion = bf16[256,2048]{1,0:T(8,128)(2,1)} fusion(bf16[512,2048]{1,0:T(8,128)(2,1)} %bitcast.90, s32[1024]{0:T(1024)S(1)} %pad_clamp_fusion), kind=kCustom, calls=%fused_computation | custom fusion | bytes 2098176 | tf_op jit(solution)/shard_map/jit(_take)/gather | solution.py:122
  181.4 2.5 %gather.7 = bf16[128,2,2048]{2,1,0:T(2,128)(2,1)} reshape(bf16[256,2048]{1,0:T(8,128)(2,1)} %gather_fusion) | data formatting | bytes 2097152 | tf_op jit(solution)/shard_map/jit(_take)/gather | solution.py:122
  184.0 5.5 %multiply_reduce_fusion = f32[128,2048]{1,0:T(8,128)S(1)} fusion(bf16[128,2,2048]{2,1,0:T(2,128)(2,1)} %gather.7, pred[128,2]{1,0:T(8,128)(4,1)S(1)} %copy.53, f32[128,2]{1,0:T(8,128)S(1)} %copy.49), kind=kLoop, calls=%fused_computation.10 | loop fusion | flops 1835008 | bytes 2098432 | tf_op jit(solution)/shard_map/reduce_sum | solution.py:123
  189.4 1.0 fusion.19
  (43 shorter events, 1.4 us)
Async XLA Ops:
  6.5 11.0 %copy-start = (bf16[512,2048]{1,0:T(8,128)(2,1)S(1)}, bf16[512,2048]{1,0:T(8,128)(2,1)}, u32[]{:S(2)}) copy-start(bf16[512,2048]{1,0:T(8,128)(2,1)} %param.16) | copy-start | bytes 6291460
  6.5 36.2 %all-gather.9.cloned.1.call-start = ((), (), s32[]{:S(2)}) async-start(), calls=%async_computation.6 | async-start | bytes 2621440 | tf_op jit(solution)/shard_map/all_gather | solution.py:80
  7.6 8.8 %collective-permute-start = (bf16[2,128,256]{2,1,0:T(8,128)(2,1)S(1)}, bf16[2,128,256]{2,1,0:T(8,128)(2,1)S(1)}, u32[]{:S(2)}, u32[]{:S(2)}) collective-permute-start(bf16[2,128,256]{2,1,0:T(8,128)(2,1)S(1)} %pad_maximum_fusion), channel_id=1, source_target_pairs={{0,4},{4,8},{8,12},{12,16},{16,20},{20,24},{24,28},{1,5},{5,9},{9,... | collective-permute-start | bytes 393224 | tf_op jit(solution)/shard_map/ppermute | solution.py:15
  17.3 1.7 copy-start.2
  18.9 25.9 %copy-start.1 = (bf16[128,2048]{1,0:T(8,128)(2,1)S(1)}, bf16[128,2048]{1,0:T(8,128)(2,1)}, u32[]{:S(2)}) copy-start(bf16[128,2048]{1,0:T(8,128)(2,1)} %param.17) | copy-start | bytes 1572868
  18.9 68.1 %all-gather.5.cloned.1.call-start = ((), (), s32[]{:S(2)}) async-start(), calls=%async_computation.3 | async-start | bytes 2621440 | tf_op jit(solution)/shard_map/all_gather | solution.py:109
  19.2 25.8 %copy-start.3 = (f32[2048]{0:T(1024)S(1)}, f32[2048]{0:T(1024)}, u32[]{:S(2)}) copy-start(f32[2048]{0:T(1024)} %param.18) | copy-start | bytes 24580
  66.2 69.2 %reduce-scatter.2.cloned.1.call-start = ((), (), s32[]{:S(2)}) async-start(), calls=%async_computation.4 | async-start | bytes 2621440 | tf_op jit(solution)/shard_map/reduce_scatter | solution.py:116
  104.0 51.8 %copy-start.4 = (f32[128,2]{0,1:T(2,128)S(1)}, f32[128,2]{0,1:T(2,128)}, u32[]{:S(2)}) copy-start(f32[128,2]{0,1:T(2,128)} %param.20) | copy-start | bytes 3076
  104.1 72.1 %all-gather.7.cloned.1.call-start = ((), (), s32[]{:S(2)}) async-start(), calls=%async_computation.5 | async-start | bytes 2621440 | tf_op jit(solution)/shard_map/all_gather | solution.py:120
Sparse Core Ops, SparseCore 0:
  19.0 23.6 all-gather.8
  66.3 20.6 all-gather.4
  104.2 31.1 reduce-scatter.1
  155.5 20.6 all-gather.6
